TPU v7x, 32 devices: a whole 2x2x4 slice. The times are simulated.
32 devices in a mesh: fs: 8 (over z, x), tp: 4 (over y, core).
Axes of the slice: x: 2, y: 2, z: 4, core: 2. Of those that a mesh axis runs over, the one named last changes fastest.
Arguments:
- later_in: bfloat16 [8192, 2048], P('fs'), may hold values from -3 to 3
- earlier_in: bfloat16 [8192, 2048], P('fs'), may hold values from -3 to 3
- cotangent: bfloat16 [8192, 2048], P('fs'), may hold values from -6 to 6
- gate_weight: bfloat16 [2048, 5632], P('fs', 'tp'), may hold values from -0.125 to 0.125
- up_weight: bfloat16 [2048, 5632], P('fs', 'tp'), may hold values from -0.125 to 0.125
- down_weight: bfloat16 [2048, 5632], P('fs', 'tp'), may hold values from -0.078125 to 0.078125
- norm_gain: bfloat16 [2048], replicated, may hold values from 0.099609375 to 1.8984375
- gate_sum: float32 [2048, 5632], P('fs', 'tp'), may hold values from -96 to 96
- up_sum: float32 [2048, 5632], P('fs', 'tp'), may hold values from -96 to 96
- down_sum: float32 [2048, 5632], P('fs', 'tp'), may hold values from -96 to 96
- gain_sum: float32 [2048], replicated, may hold values from -192 to 192
Outputs:
- later_out: bfloat16 [8192, 2048], P(('fs', 'tp'))
- later_hidden: bfloat16 [8192, 5632], P('fs', 'tp')
- earlier_grad: bfloat16 [8192, 2048], P(('fs', 'tp'))
- gate_sum_new: float32 [2048, 5632], P('fs', 'tp')
- up_sum_new: float32 [2048, 5632], P('fs', 'tp')
- down_sum_new: float32 [2048, 5632], P('fs', 'tp')
- gain_sum_new: float32 [2048], replicated
All inputs are finite; a program needn't handle non-finite values.
Results may differ from a plain program's by a relative error of at most 0.013.
Values may be sent and summed in bfloat16 or wider, within the bound.
No kernel may reach another device: no remote copies, remote signals or barrier semaphores. Data moves between devices by JAX's collectives and lax.ppermute only.
A program may use at most 128 MiB of HBM per device.

v0:
```python
import jax
import jax.numpy as jnp
from jax import lax
from jax.sharding import PartitionSpec as P

norm_floor = 0.05


def normalize(tokens_in, norm_gain):
    values = tokens_in.astype(jnp.float32)
    row_scale = lax.rsqrt(jnp.mean(values * values, axis=1, keepdims=True) + norm_floor)
    unit_rows = values * row_scale
    normed = (unit_rows * norm_gain.astype(jnp.float32)).astype(jnp.bfloat16)
    return (row_scale, unit_rows, normed)


def transposed(matrix_a, matrix_b):
    return lax.dot_general(
        matrix_a, matrix_b, (((1,), (1,)), ((), ())), preferred_element_type=jnp.float32
    )


def outer_sum(matrix_a, matrix_b):
    return lax.dot_general(
        matrix_a, matrix_b, (((0,), (0,)), ((), ())), preferred_element_type=jnp.float32
    )


def own_rows(tokens_in, own_count):
    return lax.dynamic_slice_in_dim(tokens_in, lax.axis_index("tp") * own_count, own_count, 0)


def forward(later_in, norm_gain, weights):
    w_gate, w_up, w_down = weights
    normed = normalize(later_in, norm_gain)[2]
    gate_pre = jnp.dot(normed, w_gate, preferred_element_type=jnp.float32)
    up_pre = jnp.dot(normed, w_up, preferred_element_type=jnp.float32)
    hidden = (jax.nn.silu(gate_pre) * up_pre).astype(jnp.bfloat16)
    own_count = later_in.shape[0] // lax.axis_size("tp")
    summed = lax.psum_scatter(
        transposed(hidden, w_down).astype(jnp.bfloat16), "tp", scatter_dimension=0, tiled=True
    ).astype(jnp.float32)
    later_out = (own_rows(later_in, own_count).astype(jnp.float32) + 0.5 * summed).astype(
        jnp.bfloat16
    )
    return (later_out, hidden)


def backward(earlier_in, cotangent, norm_gain, weights):
    w_gate, w_up, w_down = weights
    row_scale, unit_rows, normed = normalize(earlier_in, norm_gain)
    gate_pre = jnp.dot(normed, w_gate, preferred_element_type=jnp.float32)
    up_pre = jnp.dot(normed, w_up, preferred_element_type=jnp.float32)
    sigmoid_gate = jax.nn.sigmoid(gate_pre)
    activated = gate_pre * sigmoid_gate
    hidden = (activated * up_pre).astype(jnp.bfloat16)
    col_width = hidden.shape[1]
    dhidden = jnp.dot(cotangent, w_down, preferred_element_type=jnp.float32)
    dgate = (
        0.5 * dhidden * up_pre * sigmoid_gate * (1.0 + gate_pre * (1.0 - sigmoid_gate))
    ).astype(jnp.bfloat16)
    dupper = (0.5 * dhidden * activated).astype(jnp.bfloat16)
    gate_and_up = jnp.concatenate([dgate, dupper], axis=1)
    dnormed = transposed(dgate, w_gate) + transposed(dupper, w_up)
    gain_part = jnp.sum(dnormed * unit_rows, axis=0)
    weighted = dnormed * norm_gain.astype(jnp.float32)
    branch = row_scale * (
        weighted - unit_rows * jnp.mean(weighted * unit_rows, axis=1, keepdims=True)
    )
    own_count = earlier_in.shape[0] // lax.axis_size("tp")
    summed = lax.psum_scatter(
        branch.astype(jnp.bfloat16), "tp", scatter_dimension=0, tiled=True
    ).astype(jnp.float32)
    earlier_grad = (own_rows(cotangent, own_count).astype(jnp.float32) + summed).astype(
        jnp.bfloat16
    )
    grads_total = lax.psum_scatter(
        jnp.concatenate(
            [outer_sum(normed, gate_and_up), 0.5 * outer_sum(cotangent, hidden)], axis=1
        ).astype(jnp.bfloat16),
        "fs",
        scatter_dimension=0,
        tiled=True,
    ).astype(jnp.float32)
    grad_gate = grads_total[:, :col_width]
    grad_up = grads_total[:, col_width : 2 * col_width]
    grad_down = grads_total[:, 2 * col_width :]
    gain_total = lax.psum(gain_part, ("fs", "tp"))
    return (earlier_grad, grad_gate, grad_up, grad_down, gain_total)


def local(
    later_in,
    earlier_in,
    cotangent,
    gate_weight,
    up_weight,
    down_weight,
    norm_gain,
    gate_sum,
    up_sum,
    down_sum,
    gain_sum,
):
    pieces = (gate_weight, up_weight, down_weight)
    later_out, later_hidden = forward(
        later_in,
        norm_gain,
        (
            lax.all_gather(pieces[0], "fs", axis=0, tiled=True),
            lax.all_gather(pieces[1], "fs", axis=0, tiled=True),
            lax.all_gather(pieces[2], "fs", axis=0, tiled=True),
        ),
    )
    earlier = backward(
        earlier_in,
        cotangent,
        norm_gain,
        (
            lax.all_gather(pieces[0], "fs", axis=0, tiled=True),
            lax.all_gather(pieces[1], "fs", axis=0, tiled=True),
            lax.all_gather(pieces[2], "fs", axis=0, tiled=True),
        ),
    )
    earlier_grad, grad_gate, grad_up, grad_down, gain_total = earlier
    return (
        later_out,
        later_hidden,
        earlier_grad,
        gate_sum + grad_gate,
        up_sum + grad_up,
        down_sum + grad_down,
        gain_sum + gain_total,
    )


def solution(mesh):
    placed = (
        P("fs", None),
        P("fs", None),
        P("fs", None),
        P("fs", "tp"),
        P("fs", "tp"),
        P("fs", "tp"),
        P(),
        P("fs", "tp"),
        P("fs", "tp"),
        P("fs", "tp"),
        P(),
    )
    return jax.shard_map(
        local,
        mesh=mesh,
        in_specs=placed,
        out_specs=(
            P(("fs", "tp"), None),
            P("fs", "tp"),
            P(("fs", "tp"), None),
            P("fs", "tp"),
            P("fs", "tp"),
            P("fs", "tp"),
            P(),
        ),
        check_vma=False,
    )
```

profile of v0, /device:TPU:0, one launch (start us, length us, event | category | flops | bytes accessed | tf_op | source)
XLA Modules:
  0.0 708.4 jit_solution(3213249192349217438)
XLA Ops:
  7.2 0.0 all-gather.4.cloned.1.call-start
  7.2 0.7 all-gather.4.cloned.1.call-update
  7.9 0.0 all-gather.6.cloned.1.call-start
  7.9 0.7 all-gather.6.cloned.1.call-update
  8.7 0.0 all-gather.8.cloned.1.call-start
  8.7 0.7 all-gather.8.cloned.1.call-update
  9.4 0.0 reduce-scatter.4.cloned.1.call-start
  9.4 0.0 copy-start
  9.4 0.8 convert_element_type.59
  10.3 3.3 fusion.4
  13.6 0.0 copy-done
  13.6 0.9 fusion.13
  14.5 90.8 %all-gather.4.cloned.1.call-done = bf16[2048,1408]{1,0:T(8,128)(2,1)} async-done(((bf16[256,1408]{1,0:T(8,128)(2,1)}), bf16[2048,1408]{1,0:T(8,128)(2,1)}) %all-gather.4.cloned.1.call-update) | async-done | bytes 5767184 | tf_op jit(solution)/shard_map/all_gather | solution.py:110
  105.2 12.0 %fusion.20 = f32[1024,1408]{1,0:T(8,128)} fusion(bf16[2048,1408]{1,0:T(8,128)(2,1)} %all-gather.4.cloned.1.call-done, bf16[1024,2048]{1,0:T(8,128)(2,1)} %param.11, f32[2048]{0:T(1024)S(1)} %convert_element_type.59, f32[1024]{0:T(1024)S(1)} %add_rsqrt_fusion.1), kind=kOutput, calls=%fused_computation.38 | convolution fusion | flops 5913968640 | bytes 15740928 | tf_op jit(solution)/shard_map/dot_general | solution.py:36
  117.2 80.8 %all-gather.6.cloned.1.call-done = bf16[2048,1408]{1,0:T(8,128)(2,1)} async-done(((bf16[256,1408]{1,0:T(8,128)(2,1)}), bf16[2048,1408]{1,0:T(8,128)(2,1)}) %all-gather.6.cloned.1.call-update) | async-done | bytes 5767184 | tf_op jit(solution)/shard_map/all_gather | solution.py:111
  197.9 11.3 %multiply_convert_fusion.4 = bf16[1024,1408]{1,0:T(8,128)(2,1)S(1)} fusion(f32[1024,1408]{1,0:T(8,128)} %fusion.20, bf16[2048,1408]{1,0:T(8,128)(2,1)} %all-gather.6.cloned.1.call-done, bf16[1024,2048]{1,0:T(8,128)(2,1)} %param.11, f32[2048]{0:T(1024)S(1)} %convert_element_type.59, f32[1024]{0:T(1024)S(1)} %add_rsqrt_fusion.1), kind=kOutput, calls=%fused_computation.30 | convolution fusion | flops 5922619392 | bytes 18624512 | tf_op jit(solution)/shard_map/dot_general | solution.py:37
  209.2 0.0 copy-start.8
  209.3 81.4 %all-gather.8.cloned.1.call-done = bf16[2048,1408]{1,0:T(8,128)(2,1)} async-done(((bf16[256,1408]{1,0:T(8,128)(2,1)}), bf16[2048,1408]{1,0:T(8,128)(2,1)}) %all-gather.8.cloned.1.call-update) | async-done | bytes 5767184 | tf_op jit(solution)/shard_map/all_gather | solution.py:112
  290.6 10.9 %convolution_convert_fusion.1 = bf16[1024,2048]{1,0:T(8,128)(2,1)} fusion(bf16[1024,1408]{1,0:T(8,128)(2,1)S(1)} %multiply_convert_fusion.4, bf16[2048,1408]{1,0:T(8,128)(2,1)} %all-gather.8.cloned.1.call-done), kind=kOutput, calls=%fused_computation.32 | convolution fusion | flops 5907677184 | bytes 12845056 | tf_op jit(solution)/shard_map/dot_general | solution.py:18
  301.5 0.0 copy-done.8
  301.5 0.0 reduce-scatter.4.cloned.1.call-update
  301.5 0.2 reduce-scatter.6.cloned.1.call-start
  301.8 0.0 copy-start.1
  301.8 0.0 slice-start.2
  301.8 12.1 %fusion.26 = f32[1024,1408]{1,0:T(8,128)} fusion(bf16[2048,1408]{1,0:T(8,128)(2,1)} %all-gather.4.cloned.1.call-done, bf16[1024,2048]{1,0:T(8,128)(2,1)} %param.12, f32[1024]{0:T(1024)S(1)} %add_rsqrt_fusion, f32[2048]{0:T(1024)S(1)} %convert_element_type.59), kind=kOutput, calls=%fused_computation.44 | convolution fusion | flops 5913968640 | bytes 15740928 | tf_op jit(solution)/shard_map/dot_general | solution.py:52
  313.9 0.0 copy-done.1
  313.9 0.0 copy-start.6
  313.9 0.0 slice-start.3
  313.9 0.0 slice-start
  313.9 10.7 %fusion.28 = f32[1024,1408]{1,0:T(8,128)} fusion(bf16[2048,1408]{1,0:T(8,128)(2,1)} %all-gather.6.cloned.1.call-done, bf16[1024,2048]{1,0:T(8,128)(2,1)S(1)} %copy-done.1, f32[1024]{0:T(1024)S(1)} %add_rsqrt_fusion, f32[2048]{0:T(1024)S(1)} %convert_element_type.59), kind=kOutput, calls=%fused_computation.45 | convolution fusion | flops 5913968640 | bytes 15740928 | tf_op jit(solution)/shard_map/dot_general | solution.py:53
  324.6 0.0 slice-done.2
  324.6 0.0 copy-done.6
  324.6 0.0 slice-done.3
  324.7 0.0 slice-start.1
  324.7 12.3 %multiply_convert_fusion.2 = (bf16[1024,1408]{1,0:T(8,128)(2,1)S(1)}, bf16[1024,1408]{1,0:T(8,128)(2,1)}) fusion(f32[1024,1408]{1,0:T(8,128)} %fusion.26, f32[1024,1408]{1,0:T(8,128)} %fusion.28, bf16[1024,2048]{1,0:T(8,128)(2,1)S(1)} %copy-done.6, bf16[2048,1408]{1,0:T(8,128)(2,1)S(1)} %bitcast.18), kind=kOutput, calls=%fused_computation.26 | convolution fusion | flops 5925765120 | bytes 27262976 | tf_op jit(solution)/shard_map/dot_general | solution.py:58
  337.0 0.0 slice-done
  337.0 0.0 slice-done.1
  337.0 10.2 %fusion.30 = f32[1024,2048]{1,0:T(8,128)} fusion(bf16[1024,1408]{1,0:T(8,128)(2,1)} %get-tuple-element.10, bf16[2048,1408]{1,0:T(8,128)(2,1)S(1)} %bitcast.16), kind=kOutput, calls=%fused_computation.46 | convolution fusion | flops 5905580032 | bytes 17039360 | tf_op jit(solution)/shard_map/dot_general | solution.py:18
  347.2 11.1 %fusion.12 = (f32[2048]{0:T(1024)S(1)}, f32[1024]{0:T(1024)S(1)}, f32[1024,2048]{1,0:T(8,128)S(1)}) fusion(bf16[1024,2048]{1,0:T(8,128)(2,1)S(1)} %copy-done.1, f32[1024]{0:T(1024)S(1)} %add_rsqrt_fusion, f32[2048]{0:T(1024)S(1)} %convert_element_type.59, f32[1024,2048]{1,0:T(8,128)} %fusion.30, bf16[1024,1408]{1,0:T(8,128)(2,1)S(1)} %get-tuple-element.9, ...), kind=kOutput, calls=%fused_computation.19 | convolution fusion | flops 5922354176 | bytes 29646848 | tf_op jit(solution)/shard_map/dot_general | solution.py:18
  358.3 3.5 fusion.11
  361.8 0.0 reduce-scatter.6.cloned.1.call-update
  361.9 0.0 reduce-scatter.8.cloned.1.call-start
  361.9 0.0 copy-start.2
  361.9 13.0 %fusion.14 = bf16[2048,1408]{1,0:T(8,128)(2,1)S(1)} fusion(bf16[1024,2048]{1,0:T(8,128)(2,1)} %param.13, f32[1024,1408]{1,0:T(8,128)} %fusion.28, f32[1024,1408]{1,0:T(8,128)} %fusion.26), kind=kOutput, calls=%fused_computation.21 | convolution fusion | flops 5919997952 | bytes 21495808 | tf_op jit(solution)/shard_map/dot_general | solution.py:24
  374.9 0.0 copy-done.2
  374.9 17.4 %convolution_convert_fusion = bf16[2048,2816]{1,0:T(8,128)(2,1)} fusion(bf16[1024,1408]{1,0:T(8,128)(2,1)S(1)} %get-tuple-element.9, bf16[1024,1408]{1,0:T(8,128)(2,1)} %get-tuple-element.10, bf16[1024,2048]{1,0:T(8,128)(2,1)S(1)} %copy-done.2, f32[1024]{0:T(1024)S(1)} %add_rsqrt_fusion, f32[2048]{0:T(1024)S(1)} %convert_element_type.59), kind=kOutput, calls=%fused_computation.2 | convolution fusion | flops 11836850176 | bytes 21508096 | tf_op jit(solution)/shard_map/dot_general | solution.py:24
  392.3 11.8 %pad_maximum_fusion = bf16[2048,4224]{1,0:T(8,128)(2,1)} fusion(bf16[2048,1408]{1,0:T(8,128)(2,1)S(1)} %fusion.14, bf16[2048,2816]{1,0:T(8,128)(2,1)} %convolution_convert_fusion), kind=kLoop, calls=%fused_computation | loop fusion | flops 34603008 | bytes 34603008 | tf_op jit(solution)/shard_map/concatenate | solution.py:78
  404.1 0.0 copy-start.7
  404.1 0.0 reduce-scatter.8.cloned.1.call-update
  404.1 41.4 %psum.7 = f32[2048]{0:T(1024)S(1)} all-reduce(f32[2048]{0:T(1024)S(1)} %get-tuple-element.7), channel_id=1, replica_groups=mesh['fs'=8,'tp'=4] {'fs','tp'}, use_global_device_ids=true, to_apply=%region_7.8 | all-reduce | flops 2048 | bytes 16384 | tf_op jit(solution)/shard_map/psum | solution.py:88
  445.5 0.0 copy-done.7
  445.5 0.6 add.71
  446.1 0.0 copy-start.3
  446.1 0.0 copy-start.4
  446.1 0.0 reduce-scatter.4.cloned.1.call-done
  446.1 3.1 add_convert_fusion.1
  449.2 0.0 reduce-scatter.6.cloned.1.call-done
  449.2 2.9 add_convert_fusion
  452.2 245.1 %reduce-scatter.8.cloned.1.call-done = bf16[256,4224]{1,0:T(8,128)(2,1)} async-done(((bf16[2048,4224]{1,0:T(8,128)(2,1)}), bf16[256,4224]{1,0:T(8,128)(2,1)}) %reduce-scatter.8.cloned.1.call-update) | async-done | bytes 2162704 | tf_op jit(solution)/shard_map/reduce_scatter | solution.py:77
  697.2 2.0 convert_element_type.74
  699.2 0.0 copy-done.3
  699.2 0.0 copy-done.4
  699.3 0.0 copy-done.5
  699.3 2.3 slice_add_fusion
  (6 shorter events, 0.0 us)
Async XLA Ops:
  7.2 98.1 %all-gather.4.cloned.1.call-start = ((), (), s32[]{:S(2)}) async-start(), calls=%async_computation.3 | async-start | bytes 6488064 | tf_op jit(solution)/shard_map/all_gather | solution.py:110
  7.9 190.0 %all-gather.6.cloned.1.call-start = ((), (), s32[]{:S(2)}) async-start(), calls=%async_computation.4 | async-start | bytes 6488064 | tf_op jit(solution)/shard_map/all_gather | solution.py:111
  8.7 282.0 %all-gather.8.cloned.1.call-start = ((), (), s32[]{:S(2)}) async-start(), calls=%async_computation.5 | async-start | bytes 6488064 | tf_op jit(solution)/shard_map/all_gather | solution.py:112
  9.4 436.8 %reduce-scatter.4.cloned.1.call-start = ((), (), s32[]{:S(2)}) async-start(), calls=%async_computation.6 | async-start | bytes 5242880 | tf_op jit(solution)/shard_map/reduce_scatter | solution.py:40
  9.4 4.1 copy-start
  209.2 92.3 %copy-start.8 = (bf16[1024,1408]{1,0:T(8,128)(2,1)}, bf16[1024,1408]{1,0:T(8,128)(2,1)S(1)}, u32[]{:S(2)}) copy-start(bf16[1024,1408]{1,0:T(8,128)(2,1)S(1)} %multiply_convert_fusion.4) | copy-start | bytes 8650756
  301.5 147.7 %reduce-scatter.6.cloned.1.call-start = ((), (), s32[]{:S(2)}) async-start(), calls=%async_computation.7 | async-start | bytes 5242880 | tf_op jit(solution)/shard_map/reduce_scatter | solution.py:71
  301.8 12.2 %copy-start.1 = (bf16[1024,2048]{1,0:T(8,128)(2,1)S(1)}, bf16[1024,2048]{1,0:T(8,128)(2,1)}, u32[]{:S(2)}) copy-start(bf16[1024,2048]{1,0:T(8,128)(2,1)} %param.12) | copy-start | bytes 12582916
  301.8 22.9 %slice-start.2 = ((s8[5767168]{0:T(1024)(128)(4,1)}), s8[4194304]{0:T(1024)(128)(4,1)S(1)}, s32[]{:S(2)}) async-start(s8[5767168]{0:T(1024)(128)(4,1)} %bitcast.17), calls=%async_computation.11 | async-start | bytes 8388608
  313.9 10.7 %copy-start.6 = (bf16[1024,2048]{1,0:T(8,128)(2,1)S(1)}, bf16[1024,2048]{1,0:T(8,128)(2,1)}, u32[]{:S(2)}) copy-start(bf16[1024,2048]{1,0:T(8,128)(2,1)} %param.13) | copy-start | bytes 12582916
  313.9 10.7 %slice-start.3 = ((s8[5767168]{0:T(1024)(128)(4,1)}), s8[1572864]{0:T(1024)(128)(4,1)S(1)}, s32[]{:S(2)}) async-start(s8[5767168]{0:T(1024)(128)(4,1)} %bitcast.17), calls=%async_computation.12 | async-start | bytes 3145728
  313.9 23.0 %slice-start = ((s8[5767168]{0:T(1024)(128)(4,1)}), s8[4194304]{0:T(1024)(128)(4,1)S(1)}, s32[]{:S(2)}) async-start(s8[5767168]{0:T(1024)(128)(4,1)} %bitcast.15), calls=%async_computation.9 | async-start | bytes 8388608
  324.7 12.3 %slice-start.1 = ((s8[5767168]{0:T(1024)(128)(4,1)}), s8[1572864]{0:T(1024)(128)(4,1)S(1)}, s32[]{:S(2)}) async-start(s8[5767168]{0:T(1024)(128)(4,1)} %bitcast.15), calls=%async_computation.10 | async-start | bytes 3145728
  361.9 335.4 %reduce-scatter.8.cloned.1.call-start = ((), (), s32[]{:S(2)}) async-start(), calls=%async_computation.8 | async-start | bytes 19464192 | tf_op jit(solution)/shard_map/reduce_scatter | solution.py:77
  361.9 13.0 %copy-start.2 = (bf16[1024,2048]{1,0:T(8,128)(2,1)S(1)}, bf16[1024,2048]{1,0:T(8,128)(2,1)}, u32[]{:S(2)}) copy-start(bf16[1024,2048]{1,0:T(8,128)(2,1)} %param.12) | copy-start | bytes 12582916
  404.1 41.5 %copy-start.7 = (f32[2048]{0:T(1024)S(1)}, f32[2048]{0:T(1024)}, u32[]{:S(2)}) copy-start(f32[2048]{0:T(1024)} %param.21) | copy-start | bytes 24580
  446.1 253.1 %copy-start.3 = (f32[256,1408]{1,0:T(8,128)S(1)}, f32[256,1408]{1,0:T(8,128)}, u32[]{:S(2)}) copy-start(f32[256,1408]{1,0:T(8,128)} %param.20) | copy-start | bytes 4325380
  446.1 253.1 %copy-start.4 = (f32[256,1408]{1,0:T(8,128)S(1)}, f32[256,1408]{1,0:T(8,128)}, u32[]{:S(2)}) copy-start(f32[256,1408]{1,0:T(8,128)} %param.19) | copy-start | bytes 4325380
  697.2 2.0 copy-start.5
Sparse Core Ops, SparseCore 0:
  10.2 95.0 all-gather.3
  107.4 90.4 all-gather.5
  200.1 90.4 all-gather.7
  301.6 42.7 reduce-scatter.3
  362.0 42.7 reduce-scatter.5
  408.6 288.6 reduce-scatter.7
where the time goes:
time: 709 us; the launch traced here: 708 us
  waiting for transfers between devices  500 us (71%)
  matrix products  121 us (17%)
  blocking collectives  41.4 us (6%)
  other arithmetic  31.1 us (4%)
  between operations  14.3 us (2%)
    reduce_scatter x1, waiting for transfers between devices, backward(): lax.psum_scatter(jnp.concatenate([outer_sum(normed, gate_and_up), 0.5 * o...  245 us
    all_gather x1, waiting for transfers between devices, local(): lax.all_gather(pieces[0], 'fs', axis=0, tiled=True)  90.8 us
    all_gather x1, waiting for transfers between devices, local(): lax.all_gather(pieces[2], 'fs', axis=0, tiled=True)  81.4 us
    all_gather x1, waiting for transfers between devices, local(): lax.all_gather(pieces[1], 'fs', axis=0, tiled=True)  80.8 us
    psum x1, blocking collectives, backward(): gain_total = lax.psum(gain_part, ('fs', 'tp'))  41.4 us
    dot_general x3, matrix products, transposed(): lax.dot_general(matrix_a, matrix_b, (((1,), (1,)), ((), ())), preferred_e...  32.2 us
    dot_general x2, matrix products, outer_sum(): lax.dot_general(matrix_a, matrix_b, (((0,), (0,)), ((), ())), preferred_e...  30.4 us
  transfers between devices with their start and end apart: 6, of which 4 were waited for; matrix products, arithmetic and copies ran while one was open for 19% of the time, Pallas kernels for 0%

commit v1 on v0

--- a/solution.py
+++ b/solution.py
@@ -85,7 +85,7 @@
     grad_gate = grads_total[:, :col_width]
     grad_up = grads_total[:, col_width : 2 * col_width]
     grad_down = grads_total[:, 2 * col_width :]
-    gain_total = lax.psum(gain_part, ("fs", "tp"))
+    gain_total = jnp.sum(lax.all_gather(gain_part, ("fs", "tp")), axis=0)
     return (earlier_grad, grad_gate, grad_up, grad_down, gain_total)
 
 

time: 709 us -> 708 us (level)
    psum x1 -> x0, blocking collectives: 41.4 us -> none  [backward(): gain_total = lax.psum(gain_part, ('fs', 'tp'))]
    all_gather x0 -> x1, blocking collectives: none -> 40.9 us  [backward(): gain_total = jnp.sum(lax.all_gather(gain_part, ('fs', 'tp')), axis=0)]
where the time goes in v1:
time: 708 us
  waiting for transfers between devices  500 us (71%)
  matrix products  120 us (17%)
  blocking collectives  40.9 us (6%)
  other arithmetic  31.1 us (4%)
  between operations  14.3 us (2%)
    reduce_scatter x1, waiting for transfers between devices, backward(): lax.psum_scatter(jnp.concatenate([outer_sum(normed, gate_and_up), 0.5 * o...  245 us
    all_gather x1, waiting for transfers between devices, local(): lax.all_gather(pieces[0], 'fs', axis=0, tiled=True)  90.8 us
    all_gather x1, waiting for transfers between devices, local(): lax.all_gather(pieces[2], 'fs', axis=0, tiled=True)  81.4 us
    all_gather x1, waiting for transfers between devices, local(): lax.all_gather(pieces[1], 'fs', axis=0, tiled=True)  80.8 us
    all_gather x1, blocking collectives, backward(): gain_total = jnp.sum(lax.all_gather(gain_part, ('fs', 'tp')), axis=0)  40.9 us
    dot_general x3, matrix products, transposed(): lax.dot_general(matrix_a, matrix_b, (((1,), (1,)), ((), ())), preferred_e...  32.1 us
    dot_general x2, matrix products, outer_sum(): lax.dot_general(matrix_a, matrix_b, (((0,), (0,)), ((), ())), preferred_e...  29.9 us
  transfers between devices with their start and end apart: 6, of which 4 were waited for; matrix products, arithmetic and copies ran while one was open for 19% of the time, Pallas kernels for 0%

profile of v1, /device:TPU:0, one launch (start us, length us, event | category | flops | bytes accessed | tf_op | source)
XLA Modules:
  0.0 707.5 jit_solution(12725325519416846717)
XLA Ops:
  7.2 0.0 all-gather.5.cloned.1.call-start
  7.2 0.7 all-gather.5.cloned.1.call-update
  7.9 0.0 all-gather.7.cloned.1.call-start
  7.9 0.7 all-gather.7.cloned.1.call-update
  8.7 0.0 all-gather.9.cloned.1.call-start
  8.7 0.7 all-gather.9.cloned.1.call-update
  9.4 0.0 reduce-scatter.4.cloned.1.call-start
  9.4 0.0 copy-start
  9.4 0.8 convert_element_type.59
  10.3 3.3 fusion.4
  13.6 0.0 copy-done
  13.6 0.9 fusion.13
  14.5 90.8 %all-gather.5.cloned.1.call-done = bf16[2048,1408]{1,0:T(8,128)(2,1)} async-done(((bf16[256,1408]{1,0:T(8,128)(2,1)}), bf16[2048,1408]{1,0:T(8,128)(2,1)}) %all-gather.5.cloned.1.call-update) | async-done | bytes 5767184 | tf_op jit(solution)/shard_map/all_gather | solution.py:110
  105.2 12.0 %fusion.20 = f32[1024,1408]{1,0:T(8,128)} fusion(bf16[2048,1408]{1,0:T(8,128)(2,1)} %all-gather.5.cloned.1.call-done, bf16[1024,2048]{1,0:T(8,128)(2,1)} %param.11, f32[2048]{0:T(1024)S(1)} %convert_element_type.59, f32[1024]{0:T(1024)S(1)} %add_rsqrt_fusion.1), kind=kOutput, calls=%fused_computation.38 | convolution fusion | flops 5913968640 | bytes 15740928 | tf_op jit(solution)/shard_map/dot_general | solution.py:36
  117.2 80.8 %all-gather.7.cloned.1.call-done = bf16[2048,1408]{1,0:T(8,128)(2,1)} async-done(((bf16[256,1408]{1,0:T(8,128)(2,1)}), bf16[2048,1408]{1,0:T(8,128)(2,1)}) %all-gather.7.cloned.1.call-update) | async-done | bytes 5767184 | tf_op jit(solution)/shard_map/all_gather | solution.py:111
  197.9 11.3 %multiply_convert_fusion.4 = bf16[1024,1408]{1,0:T(8,128)(2,1)S(1)} fusion(f32[1024,1408]{1,0:T(8,128)} %fusion.20, bf16[2048,1408]{1,0:T(8,128)(2,1)} %all-gather.7.cloned.1.call-done, bf16[1024,2048]{1,0:T(8,128)(2,1)} %param.11, f32[2048]{0:T(1024)S(1)} %convert_element_type.59, f32[1024]{0:T(1024)S(1)} %add_rsqrt_fusion.1), kind=kOutput, calls=%fused_computation.30 | convolution fusion | flops 5922619392 | bytes 18624512 | tf_op jit(solution)/shard_map/dot_general | solution.py:37
  209.2 0.0 copy-start.8
  209.3 81.4 %all-gather.9.cloned.1.call-done = bf16[2048,1408]{1,0:T(8,128)(2,1)} async-done(((bf16[256,1408]{1,0:T(8,128)(2,1)}), bf16[2048,1408]{1,0:T(8,128)(2,1)}) %all-gather.9.cloned.1.call-update) | async-done | bytes 5767184 | tf_op jit(solution)/shard_map/all_gather | solution.py:112
  290.6 10.9 %convolution_convert_fusion.1 = bf16[1024,2048]{1,0:T(8,128)(2,1)} fusion(bf16[1024,1408]{1,0:T(8,128)(2,1)S(1)} %multiply_convert_fusion.4, bf16[2048,1408]{1,0:T(8,128)(2,1)} %all-gather.9.cloned.1.call-done), kind=kOutput, calls=%fused_computation.32 | convolution fusion | flops 5907677184 | bytes 12845056 | tf_op jit(solution)/shard_map/dot_general | solution.py:18
  301.5 0.0 copy-done.8
  301.5 0.0 reduce-scatter.4.cloned.1.call-update
  301.5 0.2 reduce-scatter.6.cloned.1.call-start
  301.8 0.0 copy-start.1
  301.8 0.0 slice-start.2
  301.8 12.1 %fusion.26 = f32[1024,1408]{1,0:T(8,128)} fusion(bf16[2048,1408]{1,0:T(8,128)(2,1)} %all-gather.5.cloned.1.call-done, bf16[1024,2048]{1,0:T(8,128)(2,1)} %param.12, f32[1024]{0:T(1024)S(1)} %add_rsqrt_fusion, f32[2048]{0:T(1024)S(1)} %convert_element_type.59), kind=kOutput, calls=%fused_computation.44 | convolution fusion | flops 5913968640 | bytes 15740928 | tf_op jit(solution)/shard_map/dot_general | solution.py:52
  313.9 0.0 copy-done.1
  313.9 0.0 copy-start.6
  313.9 0.0 slice-start.3
  313.9 0.0 slice-start
  313.9 10.7 %fusion.28 = f32[1024,1408]{1,0:T(8,128)} fusion(bf16[2048,1408]{1,0:T(8,128)(2,1)} %all-gather.7.cloned.1.call-done, bf16[1024,2048]{1,0:T(8,128)(2,1)S(1)} %copy-done.1, f32[1024]{0:T(1024)S(1)} %add_rsqrt_fusion, f32[2048]{0:T(1024)S(1)} %convert_element_type.59), kind=kOutput, calls=%fused_computation.45 | convolution fusion | flops 5913968640 | bytes 15740928 | tf_op jit(solution)/shard_map/dot_general | solution.py:53
  324.6 0.0 slice-done.2
  324.6 0.0 copy-done.6
  324.6 0.0 slice-done.3
  324.7 0.0 slice-start.1
  324.7 12.3 %multiply_convert_fusion.2 = (bf16[1024,1408]{1,0:T(8,128)(2,1)S(1)}, bf16[1024,1408]{1,0:T(8,128)(2,1)}) fusion(f32[1024,1408]{1,0:T(8,128)} %fusion.26, f32[1024,1408]{1,0:T(8,128)} %fusion.28, bf16[1024,2048]{1,0:T(8,128)(2,1)S(1)} %copy-done.6, bf16[2048,1408]{1,0:T(8,128)(2,1)S(1)} %bitcast.18), kind=kOutput, calls=%fused_computation.26 | convolution fusion | flops 5925765120 | bytes 27262976 | tf_op jit(solution)/shard_map/dot_general | solution.py:58
  337.0 0.0 slice-done
  337.0 0.0 slice-done.1
  337.0 10.2 %fusion.30 = f32[1024,2048]{1,0:T(8,128)} fusion(bf16[1024,1408]{1,0:T(8,128)(2,1)} %get-tuple-element.10, bf16[2048,1408]{1,0:T(8,128)(2,1)S(1)} %bitcast.16), kind=kOutput, calls=%fused_computation.46 | convolution fusion | flops 5905580032 | bytes 17039360 | tf_op jit(solution)/shard_map/dot_general | solution.py:18
  347.2 11.1 %fusion.12 = (f32[2048]{0:T(1024)S(1)}, f32[1024]{0:T(1024)S(1)}, f32[1024,2048]{1,0:T(8,128)S(1)}) fusion(bf16[1024,2048]{1,0:T(8,128)(2,1)S(1)} %copy-done.1, f32[1024]{0:T(1024)S(1)} %add_rsqrt_fusion, f32[2048]{0:T(1024)S(1)} %convert_element_type.59, f32[1024,2048]{1,0:T(8,128)} %fusion.30, bf16[1024,1408]{1,0:T(8,128)(2,1)S(1)} %get-tuple-element.9, ...), kind=kOutput, calls=%fused_computation.19 | convolution fusion | flops 5922354176 | bytes 29646848 | tf_op jit(solution)/shard_map/dot_general | solution.py:18
  358.3 3.5 fusion.11
  361.8 0.0 reduce-scatter.6.cloned.1.call-update
  361.8 0.0 reduce-scatter.8.cloned.1.call-start
  361.8 0.0 copy-start.2
  361.8 13.0 %fusion.14 = bf16[2048,1408]{1,0:T(8,128)(2,1)S(1)} fusion(bf16[1024,2048]{1,0:T(8,128)(2,1)} %param.13, f32[1024,1408]{1,0:T(8,128)} %fusion.28, f32[1024,1408]{1,0:T(8,128)} %fusion.26), kind=kOutput, calls=%fused_computation.21 | convolution fusion | flops 5919997952 | bytes 21495808 | tf_op jit(solution)/shard_map/dot_general | solution.py:24
  374.8 0.0 copy-done.2
  374.8 17.0 %convolution_convert_fusion = bf16[2048,2816]{1,0:T(8,128)(2,1)} fusion(bf16[1024,1408]{1,0:T(8,128)(2,1)S(1)} %get-tuple-element.9, bf16[1024,1408]{1,0:T(8,128)(2,1)} %get-tuple-element.10, bf16[1024,2048]{1,0:T(8,128)(2,1)S(1)} %copy-done.2, f32[1024]{0:T(1024)S(1)} %add_rsqrt_fusion, f32[2048]{0:T(1024)S(1)} %convert_element_type.59), kind=kOutput, calls=%fused_computation.2 | convolution fusion | flops 11836850176 | bytes 21508096 | tf_op jit(solution)/shard_map/dot_general | solution.py:24
  391.8 11.7 %pad_maximum_fusion = bf16[2048,4224]{1,0:T(8,128)(2,1)} fusion(bf16[2048,1408]{1,0:T(8,128)(2,1)S(1)} %fusion.14, bf16[2048,2816]{1,0:T(8,128)(2,1)} %convolution_convert_fusion), kind=kLoop, calls=%fused_computation | loop fusion | flops 34603008 | bytes 34603008 | tf_op jit(solution)/shard_map/concatenate | solution.py:78
  403.6 0.0 copy-start.7
  403.6 0.0 reduce-scatter.8.cloned.1.call-update
  403.6 40.9 %all-gather = f32[65536]{0:T(1024)S(1)} all-gather(f32[2048]{0:T(1024)S(1)} %get-tuple-element.7), channel_id=2, replica_groups=mesh['fs'=8,'tp'=4] {'fs','tp'}, dimensions={0}, use_global_device_ids=true | all-gather | bytes 270336 | tf_op jit(solution)/shard_map/all_gather | solution.py:88
  444.5 0.0 copy-done.7
  444.5 0.6 add.69
  445.1 0.0 copy-start.3
  445.1 0.0 copy-start.4
  445.2 0.0 reduce-scatter.4.cloned.1.call-done
  445.2 3.1 add_convert_fusion.1
  448.2 0.0 reduce-scatter.6.cloned.1.call-done
  448.2 2.9 add_convert_fusion
  451.1 245.3 %reduce-scatter.8.cloned.1.call-done = bf16[256,4224]{1,0:T(8,128)(2,1)} async-done(((bf16[2048,4224]{1,0:T(8,128)(2,1)}), bf16[256,4224]{1,0:T(8,128)(2,1)}) %reduce-scatter.8.cloned.1.call-update) | async-done | bytes 2162704 | tf_op jit(solution)/shard_map/reduce_scatter | solution.py:77
  696.4 2.0 convert_element_type.74
  698.4 0.0 copy-done.3
  698.4 0.0 copy-done.4
  698.4 0.0 copy-done.5
  698.4 2.3 slice_add_fusion
  (8 shorter events, 0.1 us)
Async XLA Ops:
  7.2 98.1 %all-gather.5.cloned.1.call-start = ((), (), s32[]{:S(2)}) async-start(), calls=%async_computation.3 | async-start | bytes 6488064 | tf_op jit(solution)/shard_map/all_gather | solution.py:110
  7.9 190.0 %all-gather.7.cloned.1.call-start = ((), (), s32[]{:S(2)}) async-start(), calls=%async_computation.4 | async-start | bytes 6488064 | tf_op jit(solution)/shard_map/all_gather | solution.py:111
  8.7 282.0 %all-gather.9.cloned.1.call-start = ((), (), s32[]{:S(2)}) async-start(), calls=%async_computation.5 | async-start | bytes 6488064 | tf_op jit(solution)/shard_map/all_gather | solution.py:112
  9.4 435.8 %reduce-scatter.4.cloned.1.call-start = ((), (), s32[]{:S(2)}) async-start(), calls=%async_computation.6 | async-start | bytes 5242880 | tf_op jit(solution)/shard_map/reduce_scatter | solution.py:40
  9.4 4.1 copy-start
  209.2 92.3 %copy-start.8 = (bf16[1024,1408]{1,0:T(8,128)(2,1)}, bf16[1024,1408]{1,0:T(8,128)(2,1)S(1)}, u32[]{:S(2)}) copy-start(bf16[1024,1408]{1,0:T(8,128)(2,1)S(1)} %multiply_convert_fusion.4) | copy-start | bytes 8650756
  301.5 146.7 %reduce-scatter.6.cloned.1.call-start = ((), (), s32[]{:S(2)}) async-start(), calls=%async_computation.7 | async-start | bytes 5242880 | tf_op jit(solution)/shard_map/reduce_scatter | solution.py:71
  301.8 12.2 %copy-start.1 = (bf16[1024,2048]{1,0:T(8,128)(2,1)S(1)}, bf16[1024,2048]{1,0:T(8,128)(2,1)}, u32[]{:S(2)}) copy-start(bf16[1024,2048]{1,0:T(8,128)(2,1)} %param.12) | copy-start | bytes 12582916
  301.8 22.9 %slice-start.2 = ((s8[5767168]{0:T(1024)(128)(4,1)}), s8[4194304]{0:T(1024)(128)(4,1)S(1)}, s32[]{:S(2)}) async-start(s8[5767168]{0:T(1024)(128)(4,1)} %bitcast.17), calls=%async_computation.11 | async-start | bytes 8388608
  313.9 10.7 %copy-start.6 = (bf16[1024,2048]{1,0:T(8,128)(2,1)S(1)}, bf16[1024,2048]{1,0:T(8,128)(2,1)}, u32[]{:S(2)}) copy-start(bf16[1024,2048]{1,0:T(8,128)(2,1)} %param.13) | copy-start | bytes 12582916
  313.9 10.7 %slice-start.3 = ((s8[5767168]{0:T(1024)(128)(4,1)}), s8[1572864]{0:T(1024)(128)(4,1)S(1)}, s32[]{:S(2)}) async-start(s8[5767168]{0:T(1024)(128)(4,1)} %bitcast.17), calls=%async_computation.12 | async-start | bytes 3145728
  313.9 23.0 %slice-start = ((s8[5767168]{0:T(1024)(128)(4,1)}), s8[4194304]{0:T(1024)(128)(4,1)S(1)}, s32[]{:S(2)}) async-start(s8[5767168]{0:T(1024)(128)(4,1)} %bitcast.15), calls=%async_computation.9 | async-start | bytes 8388608
  324.7 12.3 %slice-start.1 = ((s8[5767168]{0:T(1024)(128)(4,1)}), s8[1572864]{0:T(1024)(128)(4,1)S(1)}, s32[]{:S(2)}) async-start(s8[5767168]{0:T(1024)(128)(4,1)} %bitcast.15), calls=%async_computation.10 | async-start | bytes 3145728
  361.8 334.6 %reduce-scatter.8.cloned.1.call-start = ((), (), s32[]{:S(2)}) async-start(), calls=%async_computation.8 | async-start | bytes 19464192 | tf_op jit(solution)/shard_map/reduce_scatter | solution.py:77
  361.8 13.0 %copy-start.2 = (bf16[1024,2048]{1,0:T(8,128)(2,1)S(1)}, bf16[1024,2048]{1,0:T(8,128)(2,1)}, u32[]{:S(2)}) copy-start(bf16[1024,2048]{1,0:T(8,128)(2,1)} %param.12) | copy-start | bytes 12582916
  403.6 41.0 %copy-start.7 = (f32[2048]{0:T(1024)S(1)}, f32[2048]{0:T(1024)}, u32[]{:S(2)}) copy-start(f32[2048]{0:T(1024)} %param.21) | copy-start | bytes 24580
  445.1 253.3 %copy-start.3 = (f32[256,1408]{1,0:T(8,128)S(1)}, f32[256,1408]{1,0:T(8,128)}, u32[]{:S(2)}) copy-start(f32[256,1408]{1,0:T(8,128)} %param.20) | copy-start | bytes 4325380
  445.1 253.3 %copy-start.4 = (f32[256,1408]{1,0:T(8,128)S(1)}, f32[256,1408]{1,0:T(8,128)}, u32[]{:S(2)}) copy-start(f32[256,1408]{1,0:T(8,128)} %param.19) | copy-start | bytes 4325380
  696.4 2.0 copy-start.5
Sparse Core Ops, SparseCore 0:
  10.2 95.0 all-gather.4
  107.4 90.4 all-gather.6
  200.1 90.4 all-gather.8
  301.6 42.7 reduce-scatter.3
  361.9 42.7 reduce-scatter.5
  408.5 287.8 reduce-scatter.7
